TPU v7x, 32 devices: a whole 2x2x4 slice. The times are simulated.
32 devices in a mesh: sp: 16 (over z, x, core), tp: 2 (over y).
Axes of the slice: x: 2, y: 2, z: 4, core: 2. Of those that a mesh axis runs over, the one named last changes fastest.
Arguments:
- stream: bfloat16 [2048, 16384], P('tp', 'sp'), may hold values from -12 to 12
- norm_gain: float32 [2, 2048], P(None, 'tp'), may hold values from 0.1 to 1.9
- in_weight: bfloat16 [2, 2048, 1024], P(None, 'sp', 'tp'), may hold values from -0.125 to 0.125
- out_weight: bfloat16 [2, 1024, 2048], P(None, 'tp', 'sp'), may hold values from -0.1875 to 0.1875
- docs: int32 [16384], P('sp'), may hold values from 0 to 3, never falling along the last dimension, each value on 1 to 8192 neighbouring positions
Outputs:
- mixed_out: bfloat16 [2048, 16384], P('tp', 'sp')
Inputs may be any that keep to these rules, and one draw needn't show every extreme that they name: `docs`: numbers never fall along the positions and start at 0; a document spans at most 8192 positions.
All inputs are finite; a program needn't handle non-finite values.
Results may differ from a plain program's by a relative error of at most 0.0095.
Values may be sent and summed in bfloat16 or wider, within the bound.
A program may use at most 64 MiB of HBM per device.

v0:
```python
import jax
import jax.numpy as jnp
from jax import lax
from jax.sharding import PartitionSpec as P

D = 2048
PW = 1024
GROUPS = 4
WIDEST = 16
LAYERS = 2


contract_rows = (((0,), (0,)), ((), ()))


def passed_along(block, axis, distance):
    devices = range(lax.axis_size(axis))
    route = [(i - distance, i) for i in devices if i - distance in devices]
    return lax.ppermute(block, axis, route)


def trailing_pool(values, docs_own, edge_values, edge_docs, widths):
    length = values.shape[1]
    reach_back = WIDEST - 1
    extended = jnp.concatenate([edge_values, values], axis=1).astype(jnp.float32)
    ext_docs = jnp.concatenate([edge_docs, docs_own + 1])
    marker = docs_own + 1
    window_sum = jnp.zeros(values.shape, jnp.float32)
    members = jnp.zeros(values.shape, jnp.float32)
    for lag_step in range(WIDEST):
        lower_edge = reach_back - lag_step
        shifted = lax.slice_in_dim(extended, lower_edge, lower_edge + length, axis=1)
        same_doc = lax.slice_in_dim(ext_docs, lower_edge, lower_edge + length) == marker
        inside = jnp.logical_and(same_doc[None, :], lag_step < widths[:, None])
        window_sum = window_sum + jnp.where(inside, shifted, jnp.float32(0.0))
        members = members + inside.astype(jnp.float32)
    return (window_sum / members - values.astype(jnp.float32)).astype(jnp.bfloat16)


def per_device(stream, norm_gain, in_weight, out_weight, docs):
    local_rows, length = stream.shape
    pool_rows = in_weight.shape[2]
    channel = lax.axis_index("tp") * pool_rows + lax.iota(jnp.int32, pool_rows)
    widths = jnp.left_shift(jnp.int32(2), channel // (PW // GROUPS))
    residual = stream.astype(jnp.float32)
    for layer_idx in range(LAYERS):
        in_block, out_rows = (
            lax.all_gather(in_weight[layer_idx], "sp", axis=0, tiled=True),
            lax.all_gather(out_weight[layer_idx], "sp", axis=1, tiled=True),
        )
        squares = lax.psum(jnp.sum(residual * residual, axis=0), "tp")
        scaled = residual * lax.rsqrt(squares / D + 1e-06)[None, :] * norm_gain[layer_idx][:, None]
        normed = scaled.astype(jnp.bfloat16)
        pool_in = lax.dot_general(
            in_block,
            lax.all_gather(normed, "tp", axis=0, tiled=True),
            contract_rows,
            preferred_element_type=jnp.float32,
        ).astype(jnp.bfloat16)
        tail_from = length - WIDEST + 1
        edge_values, edge_docs = passed_along(
            (pool_in[:, tail_from:], docs[tail_from:] + 1), "sp", 1
        )
        pooled = trailing_pool(pool_in, docs, edge_values, edge_docs, widths)
        out_cols = lax.all_to_all(out_rows, "tp", split_axis=1, concat_axis=0, tiled=True)
        change = lax.dot_general(
            out_cols,
            lax.all_gather(pooled, "tp", axis=0, tiled=True),
            contract_rows,
            preferred_element_type=jnp.float32,
        )
        residual = residual + change
    return residual.astype(jnp.bfloat16)


def solution(mesh):
    return jax.shard_map(
        per_device,
        mesh=mesh,
        in_specs=(P("tp", "sp"), P(None, "tp"), P(None, "sp", "tp"), P(None, "tp", "sp"), P("sp")),
        out_specs=P("tp", "sp"),
        check_vma=False,
    )
```

profile of v0, /device:TPU:0, one launch (start us, length us, event | category | flops | bytes accessed | tf_op | source)
XLA Modules:
  0.0 416.0 jit_solution(8553323863351046496)
XLA Ops:
  6.5 1.8 fusion.102
  8.4 0.0 all-gather.13.cloned.1.call-start
  8.5 2.1 fusion
  10.5 5.9 %psum.14 = f32[1024]{0:T(1024)S(1)} all-reduce(f32[1024]{0:T(1024)S(1)} %fusion), channel_id=1, replica_groups=mesh['sp'=16,'tp'=2] {'tp'}, use_global_device_ids=true, to_apply=%region_1.2 | all-reduce | flops 1024 | bytes 8192 | tf_op jit(solution)/shard_map/psum | solution.py:51
  16.5 1.8 fusion.2
  18.3 0.0 all-gather.23.cloned.1.call-start
  18.4 0.6 copy-done.3
  19.0 0.1 slice_add_fusion
  19.1 1.3 collective-permute-start.1
  20.4 0.8 copy.14
  21.2 0.0 all-gather.23.cloned.1.call-update
  21.2 0.0 all-gather.15.cloned.1.call-start
  21.4 0.1 fusion.70
  21.5 32.2 %all-gather.21.cloned.1.call-done = bf16[1,2048,512]{2,1,0:T(8,128)(2,1)} async-done(((bf16[1,128,512]{2,1,0:T(8,128)(2,1)}), bf16[1,2048,512]{2,1,0:T(8,128)(2,1)}) %all-gather.21.cloned.1.call-update) | async-done | bytes 2097168 | tf_op jit(solution)/shard_map/all_gather | solution.py:48
  53.7 57.0 %all-gather.13.cloned.1.call-done = bf16[2048,1024]{1,0:T(8,128)(2,1)} async-done(((bf16[1024,1024]{1,0:T(8,128)(2,1)}), bf16[2048,1024]{1,0:T(8,128)(2,1)}) %all-gather.13.cloned.1.call-update) | async-done | bytes 4194320 | tf_op jit(solution)/shard_map/all_gather | solution.py:56
  110.7 5.2 %fusion.64 = bf16[512,1024]{0,1:T(8,128)(2,1)S(1)} fusion(bf16[2048,1024]{1,0:T(8,128)(2,1)} %all-gather.13.cloned.1.call-done, bf16[1,2048,512]{2,1,0:T(8,128)(2,1)} %all-gather.21.cloned.1.call-done), kind=kOutput, calls=%fused_computation.113 | convolution fusion | flops 2148007936 | bytes 7340032 | tf_op jit(solution)/shard_map/dot_general | solution.py:54
  116.0 1.6 collective-permute-start
  117.6 0.1 fusion.72
  117.7 0.7 collective-permute-done
  118.4 0.3 maximum_convert_fusion
  118.7 10.4 %subtract_convert_fusion.1 = bf16[512,1024]{0,1:T(8,128)(2,1)} fusion(bf16[512,1024]{0,1:T(8,128)(2,1)S(1)} %fusion.64, f32[512,1039]{0,1:T(8,128)S(1)} %maximum_convert_fusion, pred[512]{0:T(512)(128)(4,1)S(1)} %get-tuple-element.28, pred[512]{0:T(512)(128)(4,1)S(1)} %get-tuple-element.29, pred[512]{0:T(512)(128)(4,1)S(1)} %get-tuple-element.30, ...), kind=kLoop, calls=%fused_computation.109 | loop fusion | flops 41943040 | bytes 35677184 | tf_op jit(solution)/shard_map/convert_element_type | solution.py:37
  129.1 0.0 all-gather.15.cloned.1.call-update
  129.1 0.0 all-gather.25.cloned.1.call-start
  129.2 0.5 all-gather.25.cloned.1.call-update
  129.7 0.0 all-gather.17.cloned.1.call-start
  129.7 24.6 %all-gather.23.cloned.1.call-done = bf16[1,512,2048]{1,2,0:T(8,128)(2,1)} async-done(((bf16[1,512,128]{1,2,0:T(8,128)(2,1)}), bf16[1,512,2048]{1,2,0:T(8,128)(2,1)}) %all-gather.23.cloned.1.call-update) | async-done | bytes 2097168 | tf_op jit(solution)/shard_map/all_gather | solution.py:49
  154.4 52.4 %all_to_all.38 = bf16[512,2,1024]{0,2,1:T(8,128)(2,1)} all-to-all(bf16[512,2,1024]{0,2,1:T(8,128)(2,1)} %bitcast.40), channel_id=1, replica_groups=mesh['sp'=16,'tp'=2] {'tp'}, dimensions={1} | all-to-all | bytes 4194304 | tf_op jit(solution)/shard_map/all_to_all | solution.py:65
  206.8 3.9 copy.9
  210.7 6.8 %multiply_reduce_fusion = (f32[1024]{0:T(1024)S(1)}, f32[1024,1024]{1,0:T(8,128)}) fusion(bf16[1024,1024]{0,1:T(8,128)(2,1)} %all-gather.15.cloned.1.call-done, bf16[1024,1024]{1,0:T(8,128)(2,1)} %bitcast.42, bf16[1024,1024]{1,0:T(8,128)(2,1)S(1)} %copy-done), kind=kOutput, calls=%fused_computation.9 | convolution fusion | flops 2151676928 | bytes 10489856 | tf_op jit(solution)/shard_map/dot_general | solution.py:66
  217.5 4.9 %psum.15 = f32[1024]{0:T(1024)S(1)} all-reduce(f32[1024]{0:T(1024)S(1)} %get-tuple-element.26), channel_id=1, replica_groups=mesh['sp'=16,'tp'=2] {'tp'}, use_global_device_ids=true, to_apply=%region_3.4 | all-reduce | flops 1024 | bytes 8192 | tf_op jit(solution)/shard_map/psum | solution.py:51
  222.4 3.9 multiply_convert_fusion
  226.3 0.0 all-gather.17.cloned.1.call-update
  226.3 0.0 all-gather.27.cloned.1.call-start
  226.4 0.8 copy.15
  227.1 0.0 all-gather.27.cloned.1.call-update
  227.2 0.0 all-gather.19.cloned.1.call-start
  227.2 22.3 %all-gather.25.cloned.1.call-done = bf16[1,2048,512]{2,1,0:T(8,128)(2,1)} async-done(((bf16[1,128,512]{2,1,0:T(8,128)(2,1)}), bf16[1,2048,512]{2,1,0:T(8,128)(2,1)}) %all-gather.25.cloned.1.call-update) | async-done | bytes 2097168 | tf_op jit(solution)/shard_map/all_gather | solution.py:48
  249.5 56.9 %all-gather.17.cloned.1.call-done = bf16[2048,1024]{1,0:T(8,128)(2,1)} async-done(((bf16[1024,1024]{1,0:T(8,128)(2,1)}), bf16[2048,1024]{1,0:T(8,128)(2,1)}) %all-gather.17.cloned.1.call-update) | async-done | bytes 4194320 | tf_op jit(solution)/shard_map/all_gather | solution.py:56
  306.4 5.2 %fusion.61 = bf16[512,1024]{0,1:T(8,128)(2,1)S(1)} fusion(bf16[2048,1024]{1,0:T(8,128)(2,1)} %all-gather.17.cloned.1.call-done, bf16[1,2048,512]{2,1,0:T(8,128)(2,1)} %all-gather.25.cloned.1.call-done), kind=kOutput, calls=%fused_computation.112 | convolution fusion | flops 2148007936 | bytes 7340032 | tf_op jit(solution)/shard_map/dot_general | solution.py:54
  311.6 1.8 collective-permute-start.2
  313.4 0.6 collective-permute-done.2
  314.0 0.3 maximum_convert_fusion.1
  314.3 10.4 %subtract_convert_fusion = bf16[512,1024]{0,1:T(8,128)(2,1)} fusion(bf16[512,1024]{0,1:T(8,128)(2,1)S(1)} %fusion.61, f32[512,1039]{0,1:T(8,128)S(1)} %maximum_convert_fusion.1, pred[512]{0:T(512)(128)(4,1)S(1)} %get-tuple-element.28, pred[512]{0:T(512)(128)(4,1)S(1)} %get-tuple-element.29, pred[512]{0:T(512)(128)(4,1)S(1)} %get-tuple-element.30, ...), kind=kLoop, calls=%fused_computation.108 | loop fusion | flops 41943040 | bytes 35677184 | tf_op jit(solution)/shard_map/convert_element_type | solution.py:37
  324.7 25.3 %all-gather.27.cloned.1.call-done = bf16[1,512,2048]{1,2,0:T(8,128)(2,1)} async-done(((bf16[1,512,128]{1,2,0:T(8,128)(2,1)}), bf16[1,512,2048]{1,2,0:T(8,128)(2,1)}) %all-gather.27.cloned.1.call-update) | async-done | bytes 2097168 | tf_op jit(solution)/shard_map/all_gather | solution.py:49
  350.0 48.5 %all_to_all.39 = bf16[512,2,1024]{0,2,1:T(8,128)(2,1)S(1)} all-to-all(bf16[512,2,1024]{0,2,1:T(8,128)(2,1)} %bitcast.41), channel_id=1, replica_groups=mesh['sp'=16,'tp'=2] {'tp'}, dimensions={1} | all-to-all | bytes 4194304 | tf_op jit(solution)/shard_map/all_to_all | solution.py:65
  398.5 2.5 copy.11
  401.0 1.0 all-gather.19.cloned.1.call-done
  402.0 7.2 %fusion.3 = bf16[1024,1024]{1,0:T(8,128)(2,1)} fusion(f32[1024,1024]{1,0:T(8,128)} %get-tuple-element.27, bf16[1024,1024]{0,1:T(8,128)(2,1)} %all-gather.19.cloned.1.call-done, bf16[1024,1024]{1,0:T(8,128)(2,1)} %bitcast.43), kind=kOutput, calls=%fused_computation.7 | convolution fusion | flops 2149580800 | bytes 10485760 | tf_op jit(solution)/shard_map/dot_general | solution.py:66
  (29 shorter events, 0.3 us)
Async XLA Ops:
  6.5 9.9 %copy-start = (bf16[1024,1024]{1,0:T(8,128)(2,1)S(1)}, bf16[1024,1024]{1,0:T(8,128)(2,1)}, u32[]{:S(2)}) copy-start(bf16[1024,1024]{1,0:T(8,128)(2,1)} %param.5) | copy-start | bytes 6291460
  6.5 9.9 %copy-start.2 = (f32[2,1024]{1,0:T(2,128)S(1)}, f32[2,1024]{1,0:T(2,128)}, u32[]{:S(2)}) copy-start(f32[2,1024]{1,0:T(2,128)} %param.6) | copy-start | bytes 24580
  6.5 47.2 %all-gather.21.cloned.1.call-start = ((), (), s32[]{:S(2)}) async-start(), calls=%async_computation.6 | async-start | bytes 2228224 | tf_op jit(solution)/shard_map/all_gather | solution.py:48
  8.4 102.3 %all-gather.13.cloned.1.call-start = ((), (), s32[]{:S(2)}) async-start(), calls=%async_computation.2 | async-start | bytes 6291456 | tf_op jit(solution)/shard_map/all_gather | solution.py:56
  18.3 0.7 copy-start.3
  18.3 2.0 copy-start.1
  18.3 136.1 %all-gather.23.cloned.1.call-start = ((), (), s32[]{:S(2)}) async-start(), calls=%async_computation.7 | async-start | bytes 2228224 | tf_op jit(solution)/shard_map/all_gather | solution.py:49
  19.1 2.4 collective-permute-start.1
  21.2 189.5 %all-gather.15.cloned.1.call-start = ((), (), s32[]{:S(2)}) async-start(), calls=%async_computation.3 | async-start | bytes 3145728 | tf_op jit(solution)/shard_map/all_gather | solution.py:68
  116.0 2.4 collective-permute-start
  129.1 120.4 %all-gather.25.cloned.1.call-start = ((), (), s32[]{:S(2)}) async-start(), calls=%async_computation.8 | async-start | bytes 2228224 | tf_op jit(solution)/shard_map/all_gather | solution.py:48
  129.7 176.7 %all-gather.17.cloned.1.call-start = ((), (), s32[]{:S(2)}) async-start(), calls=%async_computation.4 | async-start | bytes 6291456 | tf_op jit(solution)/shard_map/all_gather | solution.py:56
  226.3 123.7 %all-gather.27.cloned.1.call-start = ((), (), s32[]{:S(2)}) async-start(), calls=%async_computation.9 | async-start | bytes 2228224 | tf_op jit(solution)/shard_map/all_gather | solution.py:49
  227.2 174.8 %all-gather.19.cloned.1.call-start = ((), (), s32[]{:S(2)}) async-start(), calls=%async_computation.5 | async-start | bytes 3145728 | tf_op jit(solution)/shard_map/all_gather | solution.py:68
  311.6 2.4 collective-permute-start.2
Sparse Core Ops, SparseCore 0:
  9.5 44.1 all-gather.20
  55.2 55.4 all-gather.12
  112.9 41.4 all-gather.22
  155.8 52.3 all-gather.14
  210.2 39.2 all-gather.24
  250.9 55.4 all-gather.16
  308.5 41.4 all-gather.26
  351.5 50.3 all-gather.18
where the time goes:
time: 417 us; the launch traced here: 416 us
  waiting for transfers between devices  221 us (53%)
  blocking collectives  112 us (27%)
  other arithmetic  29.6 us (7%)
  matrix products  24.4 us (6%)
  between operations  13.7 us (3%)
  local copies, waits for them, and re-layouts  10.5 us (3%)
  starting transfers between devices  4.9 us (1%)
    all_gather x2, waiting for transfers between devices, per_device(): lax.all_gather(normed, 'tp', axis=0, tiled=True)  114 us
    all_to_all x2, blocking collectives, per_device(): lax.all_to_all(out_rows, 'tp', split_axis=1, concat_axis=0, tiled=True)  101 us
    all_gather x2, waiting for transfers between devices, per_device(): lax.all_gather(in_weight[layer_idx], 'sp', axis=0, tiled=True)  54.4 us
    all_gather x2, waiting for transfers between devices, per_device(): lax.all_gather(out_weight[layer_idx], 'sp', axis=1, tiled=True)  49.9 us
    convert_element_type x2, other arithmetic, trailing_pool(): (window_sum / members - values.astype(jnp.float32)).astype(jnp.bfloat16)  20.8 us
    dot_general x2, matrix products, per_device(): lax.dot_general(out_cols, lax.all_gather(pooled, 'tp', axis=0, tiled=True...  13.9 us
    psum x2, blocking collectives, per_device(): squares = lax.psum(jnp.sum(residual * residual, axis=0), 'tp')  10.8 us
    dot_general x2, matrix products, per_device(): lax.dot_general(in_block, lax.all_gather(normed, 'tp', axis=0, tiled=True...  10.4 us
  transfers between devices with their start and end apart: 11, of which 9 were waited for; matrix products, arithmetic and copies ran while one was open for 13% of the time, Pallas kernels for 0%

commit v1 on v0

--- a/solution.py
+++ b/solution.py
@@ -1,7 +1,10 @@
 import jax
 import jax.numpy as jnp
 from jax import lax
+from jax.experimental import pallas as pl
+from jax.experimental.pallas import tpu as pltpu
 from jax.sharding import PartitionSpec as P
+import functools
 
 D = 2048
 PW = 1024
@@ -73,9 +76,377 @@
     return residual.astype(jnp.bfloat16)
 
 
+HALO = 32
+F32 = jnp.float32
+BF16 = jnp.bfloat16
+
+
+def fused_kernel(
+    nsp, stream, tails, dcol, gain, inw, outw, out,
+    bin_, bout, res, xn, pin, pooled, xrecv, ostage, hbuf, dbuf, gbuf, masks, invs,
+    lane_sem, core_sem, sent_sem, own_sem, sx, rx, so, ro, ms, mr,
+):
+    nz = nsp // 4
+    H = stream.shape[1] // 2
+    T = H + HALO
+    s, y = lax.axis_index("sp"), lax.axis_index("tp")
+    c, x, z = lax.rem(s, 2), lax.rem(s // 2, 2), s // 4
+    py = 1 - y
+    half = PW // 2
+    zw = 128
+    seg = nz * zw
+
+    def blk(k, zz, xx, cc, yy):
+        l = k // 2
+        if k % 2 == 0:
+            row = (((l * 2 + yy) * 2 + cc) * 2 + xx) * seg + zz * zw
+            return bin_.at[pl.ds(pl.multiple_of(row, zw), zw), :]
+        row = (((l * 2 + cc) * 2 + xx) * 2 + yy) * half
+        return bout.at[pl.ds(pl.multiple_of(row, half), half), pl.ds(pl.multiple_of(zz * zw, zw), zw)]
+
+    def own(k):
+        return (inw if k % 2 == 0 else outw).at[k // 2]
+
+    def rcopy(src, dst, ss, rs, sp, tp):
+        return pltpu.make_async_remote_copy(
+            src_ref=src, dst_ref=dst, send_sem=ss, recv_sem=rs,
+            device_id=(sp, tp), device_id_type=pl.DeviceIdType.MESH)
+
+    def zat(dz):
+        return lax.rem(z + dz, nz)
+
+    def rel(dx, dy, dz):
+        return (dx * 2 + dy) * nz + dz
+
+    def place(k, dx, dy, dz):
+        return blk(k, zat(dz), (x + dx) % 2 if isinstance(x, int) else lax.rem(x + dx, 2), c, lax.rem(y + dy, 2))
+
+    def source(k, dx, dy, dz):
+        return own(k) if dx == dy == dz == 0 else place(k, dx, dy, dz)
+
+    def to_z(k, dy):
+        for d in (1, nz - 1, 2) if nz == 4 else range(1, nz):
+            rcopy(source(k, 0, dy, 0), place(k, 0, dy, 0), sent_sem.at[k],
+                  lane_sem.at[k, rel(0, dy, nz - d)], zat(d) * 4 + x * 2 + c, y).start()
+
+    def to_y(k, dz):
+        rcopy(source(k, 0, 0, dz), place(k, 0, 0, dz), sent_sem.at[k],
+              lane_sem.at[k, rel(0, 1, dz)], s, py).start()
+
+    def to_x(k, dy, dz):
+        rcopy(source(k, 0, dy, dz), place(k, 0, dy, dz), sent_sem.at[k],
+              lane_sem.at[k, rel(1, dy, dz)], z * 4 + (1 - x) * 2 + c, y).start()
+
+    def to_core(k, dx, dy, dz):
+        rcopy(source(k, dx, dy, dz), place(k, dx, dy, dz), sent_sem.at[k],
+              core_sem.at[k], z * 4 + x * 2 + 1 - c, y).start()
+
+    def arrived(k, dx, dy, dz):
+        rcopy(own(k), place(k, dx, dy, dz), sent_sem.at[k],
+              lane_sem.at[k, rel(dx, dy, dz)], s, py).wait_recv()
+
+    def own_sends(k):
+        if k == 0:
+            to_y(k, 0)
+        to_z(k, 0)
+        to_x(k, 0, 0)
+        if k > 0:
+            to_y(k, 0)
+        to_core(k, 0, 0, 0)
+        pltpu.make_async_copy(own(k), place(k, 0, 0, 0), own_sem.at[k]).start()
+
+    zorder = (1, nz - 1, 2) if nz == 4 else tuple(range(1, nz))
+
+    def z_forward(k):
+        for dz in zorder:
+            arrived(k, 0, 0, dz)
+            if k > 0:
+                to_y(k, dz)
+            to_x(k, 0, dz)
+            to_core(k, 0, 0, dz)
+
+    def y_forward(k):
+        if k == 0:
+            arrived(k, 0, 1, 0)
+            to_z(k, 1)
+            to_x(k, 1, 0)
+            to_core(k, 0, 1, 0)
+            return
+        for dz in (0,) + zorder:
+            arrived(k, 0, 1, dz)
+            to_x(k, 1, dz)
+            to_core(k, 0, 1, dz)
+
+    def yz_forward(k):
+        for dz in zorder:
+            arrived(k, 0, 1, dz)
+            to_x(k, 1, dz)
+            to_core(k, 0, 1, dz)
+
+    def x_forward(k):
+        order = [(0, 0)] + ([(1, 0)] if k == 0 else [])
+        order += [(0, dz) for dz in zorder]
+        order += [(1, dz) for dz in ((0,) if k > 0 else ()) + zorder]
+        for dy, dz in order:
+            arrived(k, 1, dy, dz)
+            to_core(k, 1, dy, dz)
+
+    def bulk_wait(sem, blocks):
+        ref = bin_.at[pl.ds(0, blocks * zw), :]
+        pltpu.make_async_copy(ref, ref, sem).wait()
+
+    def finish(k):
+        pltpu.make_async_copy(own(k), place(k, 0, 0, 0), own_sem.at[k]).wait()
+        bulk_wait(core_sem.at[k], 4 * nz)
+
+    gcopy = rcopy(gain, gbuf, ms.at[3], mr.at[3], s, py)
+    t0 = rcopy(tails.at[0], hbuf.at[0], ms.at[0], mr.at[0], s, py)
+    nxt = lax.rem(s + 1, nsp)
+    t1 = [rcopy(tails.at[1], hbuf.at[h], ms.at[1], mr.at[h], nxt, 0) for h in (0, 1)]
+    L = stream.shape[1]
+    d1 = rcopy(dcol.at[pl.ds(L - HALO, HALO), :], dbuf, ms.at[2], mr.at[2], nxt, 0)
+    more = s < nsp - 1
+    own_sends(0)
+    gcopy.start()
+
+    @pl.when(y == 0)
+    def _():
+        t0.start()
+
+    for h in (0, 1):
+        @pl.when(jnp.logical_and(more, y == h))
+        def _():
+            t1[h].start()
+
+    @pl.when(jnp.logical_and(more, y == 0))
+    def _():
+        d1.start()
+
+    chunk = stream.shape[0] // 4
+    xs = [rcopy(stream.at[pl.ds(i * chunk, chunk), pl.ds(pl.multiple_of(py * H, H), H)],
+                xrecv.at[pl.ds(i * chunk, chunk), :], sx.at[i], rx.at[i], s, py) for i in range(4)]
+    for cp in xs:
+        cp.start()
+
+    nb = stream.shape[0] // zw
+
+    def col(b, h):
+        cc, xx, zz = b % 2, (b // 2) % 2, h * (nz // 2) + b // 4
+        return pl.multiple_of((cc * 2 + xx) * seg + zz * zw, zw)
+
+    def turn(block):
+        return block.astype(F32).T
+
+    y_forward(0)
+    own_sends(1)
+
+    @pl.loop(0, nb)
+    def _(b):
+        rows = pl.ds(pl.multiple_of(b * zw, zw), zw)
+        res[pl.ds(HALO, H), pl.ds(col(b, y), zw)] = turn(stream[rows, pl.ds(pl.multiple_of(y * H, H), H)])
+
+    @pl.when(y == 1)
+    def _():
+        hbuf[1] = tails[0]
+        dbuf[...] = dcol[pl.ds(H - HALO, HALO), :]
+
+    @pl.when(jnp.logical_and(y == 0, s == 0))
+    def _():
+        hbuf[...] = jnp.zeros_like(hbuf)
+        dbuf[...] = jnp.full(dbuf.shape, -1, jnp.int32)
+
+    @pl.when(jnp.logical_or(y == 1, s > 0))
+    def _():
+        rcopy(tails.at[0], hbuf.at[0], ms.at[0], mr.at[0], s, py).wait_recv()
+
+    @pl.when(jnp.logical_and(y == 0, s > 0))
+    def _():
+        rcopy(tails.at[0], hbuf.at[1], ms.at[0], mr.at[1], s, py).wait_recv()
+        d1.wait_recv()
+
+    gcopy.wait_recv()
+    docs_all = jnp.concatenate([dbuf[...], dcol[pl.ds(pl.multiple_of(y * H, H), H), :]], axis=0)
+    docs_f = docs_all.astype(F32)
+    count = jnp.ones((T, 128), F32)
+    for i in range(4):
+        same = (pltpu.roll(docs_f, 1 << i, 0) == docs_f).astype(F32)
+        masks[i] = same
+        count = count + same * pltpu.roll(count, 1 << i, 0)
+        invs[i] = 1.0 / count
+    for h in (0, 1):
+        for b in range(nb):
+            cc, xx, zz = b % 2, (b // 2) % 2, h * (nz // 2) + b // 4
+            at = (cc * 2 + xx) * seg + zz * zw
+            res[pl.ds(0, HALO), at:at + zw] = hbuf[h, :, b * zw:(b + 1) * zw].astype(F32)
+
+    z_forward(0)
+    yz_forward(0)
+    z_forward(1)
+    own_sends(2)
+    x_forward(0)
+    per = chunk // zw
+    for i in range(4):
+        xs[i].wait_recv()
+
+        @pl.loop(i * per, (i + 1) * per)
+        def _(b):
+            rows = pl.ds(pl.multiple_of(b * zw, zw), zw)
+            res[pl.ds(HALO, H), pl.ds(col(b, py), zw)] = turn(xrecv[rows, :])
+
+    def norm(l):
+        inv = lax.rsqrt(jnp.sum(res[...] * res[...], axis=1, keepdims=True) / D + 1e-06)
+        for h in (0, 1):
+            g = jnp.where(y == h, gain[l], gbuf[l])
+            for b in range(nb):
+                cc, xx, zz = b % 2, (b // 2) % 2, h * (nz // 2) + b // 4
+                at = (cc * 2 + xx) * seg + zz * zw
+                xn[:, at:at + zw] = (res[:, at:at + zw] * inv * g[b:b + 1, :]).astype(BF16)
+
+    def in_proj(l):
+        for yy in (0, 1):
+            w = bin_[pl.ds((l * 2 + yy) * 4 * seg, 4 * seg), :]
+            acc = jnp.dot(xn[...], w, preferred_element_type=F32)
+            pin[:, yy * half:(yy + 1) * half] = acc.astype(BF16).astype(F32)
+
+    def pool():
+        per_group = PW // GROUPS // 128
+        for g in range(GROUPS):
+            @pl.loop(0, per_group)
+            def _(j):
+                at = pl.ds(pl.multiple_of((g * per_group + j) * 128, 128), 128)
+                v = pin[:, at]
+                total = v
+                for i in range(g + 1):
+                    total = total + masks[i] * pltpu.roll(total, 1 << i, 0)
+                pooled[:, at] = (total * invs[g] - v).astype(BF16)
+
+    finish(0)
+    norm(0)
+    in_proj(0)
+    y_forward(1)
+    z_forward(2)
+    own_sends(3)
+    pool()
+    x_forward(1)
+    y_forward(2)
+    z_forward(3)
+    finish(1)
+
+    @pl.loop(0, 4)
+    def _(q):
+        w = bout[pl.ds(pl.multiple_of(q * PW, PW), PW), :]
+        at = pl.ds(pl.multiple_of(q * seg, seg), seg)
+        res[:, at] += jnp.dot(pooled[...], w, preferred_element_type=F32)
+
+    norm(1)
+    x_forward(2)
+    y_forward(3)
+    finish(2)
+    in_proj(1)
+    pool()
+    x_forward(3)
+    finish(3)
+    hz = nz // 2
+
+    def last(q, h):
+        cols = pl.ds(pl.multiple_of(h * hz * zw, hz * zw), hz * zw)
+        w = bout[pl.ds((4 + q) * PW, PW), cols]
+        at = pl.ds(pl.multiple_of(q * seg + h * hz * zw, hz * zw), hz * zw)
+        r = res[pl.ds(HALO, H), at] + jnp.dot(pooled[pl.ds(HALO, H), :], w, preferred_element_type=F32)
+        return r.T.astype(BF16)
+
+    sends = []
+    pending = []
+    for q in range(4):
+        v = last(q, py)
+        for cp in pending:
+            cp.start()
+        pending = []
+        for i in range(hz):
+            b = i * 4 + (q % 2) * 2 + q // 2
+            ostage[b * zw:(b + 1) * zw, :] = v[i * zw:(i + 1) * zw, :]
+            pending.append(rcopy(
+                ostage.at[pl.ds(b * zw, zw), :],
+                out.at[pl.ds(b * zw, zw), pl.ds(pl.multiple_of(y * H, H), H)],
+                so.at[b], ro.at[b], s, py))
+        sends += pending
+    for q in range(4):
+        v = last(q, y)
+        for cp in pending:
+            cp.start()
+        pending = []
+        for i in range(hz):
+            b = i * 4 + (q % 2) * 2 + q // 2
+            out[b * zw:(b + 1) * zw, pl.ds(pl.multiple_of(y * H, H), H)] = v[i * zw:(i + 1) * zw, :]
+
+    gcopy.wait_send()
+
+    @pl.when(y == 0)
+    def _():
+        t0.wait_send()
+
+    @pl.when(more)
+    def _():
+        t1[0].wait_send()
+
+    @pl.when(jnp.logical_and(more, y == 0))
+    def _():
+        d1.wait_send()
+
+    for cp in xs:
+        cp.wait_send()
+    for k in range(4):
+        bulk_wait(sent_sem.at[k], 8 * nz - 1)
+    for b in range(nb):
+        rcopy(ostage.at[pl.ds(b * zw, zw), :],
+              out.at[pl.ds(b * zw, zw), pl.ds(pl.multiple_of(py * H, H), H)],
+              so.at[b], ro.at[b], s, py).wait()
+
+
+def fused_device(nsp, stream, norm_gain, in_weight, out_weight, docs):
+    rows, L = stream.shape
+    H = L // 2
+    T = H + HALO
+    nz = nsp // 4
+    tails = jnp.stack([stream[:, H - HALO:H].T, stream[:, L - HALO:].T])
+    dcol = jnp.broadcast_to(docs[:, None], (L, 128))
+    gain = norm_gain.reshape(LAYERS, rows // 128, 128)
+    vmem = pl.BlockSpec(memory_space=pltpu.VMEM)
+    dma = pltpu.SemaphoreType.DMA
+    return pl.pallas_call(
+        functools.partial(fused_kernel, nsp),
+        out_shape=jax.ShapeDtypeStruct((rows, L), BF16),
+        in_specs=[vmem] * 6,
+        out_specs=vmem,
+        scratch_shapes=[
+            pltpu.VMEM((LAYERS * D * 2, PW // 2), BF16),
+            pltpu.VMEM((LAYERS * PW * 4, D // 4), BF16),
+            pltpu.VMEM((T, D), F32),
+            pltpu.VMEM((T, D), BF16),
+            pltpu.VMEM((T, PW), F32),
+            pltpu.VMEM((T, PW), BF16),
+            pltpu.VMEM((rows, H), BF16),
+            pltpu.VMEM((rows, H), BF16),
+            pltpu.VMEM((2, HALO, rows), BF16),
+            pltpu.VMEM((HALO, 128), jnp.int32),
+            pltpu.VMEM((LAYERS, rows // 128, 128), F32),
+            pltpu.VMEM((4, T, 128), F32),
+            pltpu.VMEM((4, T, 128), F32),
+            dma((4, 4 * nz)), dma((4,)), dma((4,)), dma((4,)),
+            dma((4,)), dma((4,)), dma((rows // 128,)), dma((rows // 128,)),
+            dma((4,)), dma((4,)),
+        ],
+        compiler_params=pltpu.CompilerParams(has_side_effects=True, vmem_limit_bytes=60 * 1024 * 1024),
+    )(stream, tails, dcol, gain, in_weight, out_weight)
+
+
 def solution(mesh):
+    nsp, ntp = mesh.shape["sp"], mesh.shape["tp"]
+    body = per_device
+    if ntp == 2 and nsp == D // 128:
+        body = functools.partial(fused_device, nsp)
     return jax.shard_map(
-        per_device,
+        body,
         mesh=mesh,
         in_specs=(P("tp", "sp"), P(None, "tp"), P(None, "sp", "tp"), P(None, "tp", "sp"), P("sp")),
         out_specs=P("tp", "sp"),

time: 417 us -> 147 us (0.35)
  waiting for transfers between devices: 221 us -> 0 us
  Pallas kernels: 0 us -> 138 us
  blocking collectives: 112 us -> 0 us
  other arithmetic: 29.6 us -> 0.69 us
  matrix products: 24.4 us -> 0 us
  between operations: 13.7 us -> 0.02 us
  starting transfers between devices: 4.9 us -> 0 us
    all_gather x8 -> x0, waiting for transfers between devices: 219 us -> none  [the longest x2 114 us: per_device(): lax.all_gather(normed, 'tp', axis=0, tiled=True)]
    pallas_call x0 -> x1, Pallas kernels: none -> 138 us  [fused_device(): pl.pallas_call(functools.partial(fused_kernel, nsp), out_shape=jax.ShapeD...]
    all_to_all x2 -> x0, blocking collectives: 101 us -> none  [per_device(): lax.all_to_all(out_rows, 'tp', split_axis=1, concat_axis=0, tiled=True)]
    convert_element_type x7 -> x0, other arithmetic: 27.2 us -> none  [the longest x2 20.8 us: trailing_pool(): (window_sum / members - values.astype(jnp.float32)).astype(jnp.bfloat16)]
    dot_general x4 -> x0, matrix products: 24.4 us -> none  [the longest x2 13.9 us: per_device(): lax.dot_general(out_cols, lax.all_gather(pooled, 'tp', axis=0, tiled=True...]
    psum x2 -> x0, blocking collectives: 10.8 us -> none  [per_device(): squares = lax.psum(jnp.sum(residual * residual, axis=0), 'tp')]
    all_to_all x2 -> x0, local copies, waits for them, and re-layouts: 6.39 us -> none  [per_device(): lax.all_to_all(out_rows, 'tp', split_axis=1, concat_axis=0, tiled=True)]
    ppermute x3 -> x0, starting transfers between devices: 4.61 us -> none  [passed_along(): return lax.ppermute(block, axis, route)]
  transfers between devices with their start and end apart: 11 -> 0, of which waited for: 9 -> 0; matrix products, arithmetic and copies ran while one was open for 13% -> 0% of each run, Pallas kernels for 0% -> 0%
where the time goes in v1:
time: 147 us; the launch traced here: 146 us
  Pallas kernels  138 us (94%)
  local copies, waits for them, and re-layouts  7.54 us (5%)
    pallas_call x1, Pallas kernels, fused_device(): pl.pallas_call(functools.partial(fused_kernel, nsp), out_shape=jax.ShapeD...  138 us
    unnamed x4, local copies, waits for them, and re-layouts  4.62 us

profile of v1, /device:TPU:0, one launch (start us, length us, event | category | flops | bytes accessed | tf_op | source)
XLA Modules:
  0.0 146.3 jit_solution(6117141633074567754)
XLA Ops:
  0.0 1.3 copy.12
  1.3 1.7 %broadcast_in_dim.2.dcol = s32[1024,128]{1,0:T(8,128)} broadcast(s32[1024]{0:T(1024)} %param.9), dimensions={0} | broadcast | bytes 528384 | tf_op jit(solution)/shard_map/broadcast_in_dim | solution.py:412
  3.0 1.2 fusion
  4.2 0.1 copy.8
  4.3 0.1 copy.9
  4.5 0.7 pad_maximum_fusion.tails
  5.2 138.1 %shard_map.55 = bf16[1024,1024]{1,0:T(8,128)(2,1)} custom-call(bf16[1024,1024]{1,0:T(8,128)(2,1)} %stream.1, bf16[2,32,1024]{2,1,0:T(8,128)(2,1)} %pad_maximum_fusion.tails, s32[1024,128]{1,0:T(8,128)} %broadcast_in_dim.2.dcol, f32[2,8,128]{2,1,0:T(8,128)} %bitcast.12, bf16[2,128,512]{2,1,0:T(8,128)(2,1)} %inw.1, bf16[2,512,128]{2,1,0:T(8,128)(2,1)} %outw.1), custom_call_target="tpu_custom_call" | custom-call | tf_op jit(solution)/shard_map/pallas_call | solution.py:416
  143.3 3.1 %copy.14 = bf16[1024,1024]{1,0:T(8,128)(2,1)} copy(bf16[1024,1024]{1,0:T(8,128)(2,1)} %shard_map.55) | data formatting | bytes 4194304

commit v2 on v1

--- a/solution.py
+++ b/solution.py
@@ -82,12 +82,13 @@
 
 
 def fused_kernel(
-    nsp, stream, tails, dcol, gain, inw, outw, out,
+    nsp, stream, tails, docs, gain, inw, outw, out,
     bin_, bout, res, xn, pin, pooled, xrecv, ostage, hbuf, dbuf, gbuf, masks, invs,
     lane_sem, core_sem, sent_sem, own_sem, sx, rx, so, ro, ms, mr,
 ):
     nz = nsp // 4
-    H = stream.shape[1] // 2
+    L = stream.shape[1]
+    H = L // 2
     T = H + HALO
     s, y = lax.axis_index("sp"), lax.axis_index("tp")
     c, x, z = lax.rem(s, 2), lax.rem(s // 2, 2), s // 4
@@ -119,7 +120,7 @@
         return (dx * 2 + dy) * nz + dz
 
     def place(k, dx, dy, dz):
-        return blk(k, zat(dz), (x + dx) % 2 if isinstance(x, int) else lax.rem(x + dx, 2), c, lax.rem(y + dy, 2))
+        return blk(k, zat(dz), lax.rem(x + dx, 2), c, lax.rem(y + dy, 2))
 
     def source(k, dx, dy, dz):
         return own(k) if dx == dy == dz == 0 else place(k, dx, dy, dz)
@@ -129,9 +130,9 @@
             rcopy(source(k, 0, dy, 0), place(k, 0, dy, 0), sent_sem.at[k],
                   lane_sem.at[k, rel(0, dy, nz - d)], zat(d) * 4 + x * 2 + c, y).start()
 
-    def to_y(k, dz):
-        rcopy(source(k, 0, 0, dz), place(k, 0, 0, dz), sent_sem.at[k],
-              lane_sem.at[k, rel(0, 1, dz)], s, py).start()
+    def to_y(k, dx, dz):
+        rcopy(source(k, dx, 0, dz), place(k, dx, 0, dz), sent_sem.at[k],
+              lane_sem.at[k, rel(dx, 1, dz)], s, py).start()
 
     def to_x(k, dy, dz):
         rcopy(source(k, 0, dy, dz), place(k, 0, dy, dz), sent_sem.at[k],
@@ -139,74 +140,92 @@
 
     def to_core(k, dx, dy, dz):
         rcopy(source(k, dx, dy, dz), place(k, dx, dy, dz), sent_sem.at[k],
-              core_sem.at[k], z * 4 + x * 2 + 1 - c, y).start()
+              core_sem.at[k, dx], z * 4 + x * 2 + 1 - c, y).start()
 
     def arrived(k, dx, dy, dz):
         rcopy(own(k), place(k, dx, dy, dz), sent_sem.at[k],
               lane_sem.at[k, rel(dx, dy, dz)], s, py).wait_recv()
 
-    def own_sends(k):
-        if k == 0:
-            to_y(k, 0)
-        to_z(k, 0)
-        to_x(k, 0, 0)
-        if k > 0:
-            to_y(k, 0)
-        to_core(k, 0, 0, 0)
+    zorder = (1, nz - 1, 2) if nz == 4 else tuple(range(1, nz))
+    x_first = {1: (1, nz - 1), 2: tuple(range(nz)), 3: ()}
+
+    def keep_own(k):
         pltpu.make_async_copy(own(k), place(k, 0, 0, 0), own_sem.at[k]).start()
 
-    zorder = (1, nz - 1, 2) if nz == 4 else tuple(range(1, nz))
-
-    def z_forward(k):
+    def first_hop(k, dz):
+        if dz:
+            arrived(k, 0, 0, dz)
+        if dz in x_first[k]:
+            to_x(k, 0, dz)
+            to_y(k, 0, dz)
+        else:
+            to_y(k, 0, dz)
+            to_x(k, 0, dz)
+        to_core(k, 0, 0, dz)
+
+    def second_hop(k):
+        for dz in (0,) + zorder:
+            if dz in x_first[k]:
+                arrived(k, 1, 0, dz)
+                to_y(k, 1, dz)
+                to_core(k, 1, 0, dz)
+            else:
+                arrived(k, 0, 1, dz)
+                to_x(k, 1, dz)
+                to_core(k, 0, 1, dz)
+
+    def third_hop(k):
+        for dz in (0,) + zorder:
+            dx, dy = (0, 1) if dz in x_first[k] else (1, 0)
+            arrived(k, dx, dy, dz)
+            to_core(k, dx, dy, dz)
+        for dz in (0,) + zorder:
+            arrived(k, 1, 1, dz)
+            to_core(k, 1, 1, dz)
+
+    def begin0():
+        to_y(0, 0, 0)
+        to_z(0, 0)
+        to_x(0, 0, 0)
+        to_core(0, 0, 0, 0)
+        keep_own(0)
+
+    def across0():
+        arrived(0, 0, 1, 0)
+        to_z(0, 1)
+        to_x(0, 1, 0)
+        to_core(0, 0, 1, 0)
+
+    def along0():
         for dz in zorder:
-            arrived(k, 0, 0, dz)
-            if k > 0:
-                to_y(k, dz)
-            to_x(k, 0, dz)
-            to_core(k, 0, 0, dz)
-
-    def y_forward(k):
-        if k == 0:
-            arrived(k, 0, 1, 0)
-            to_z(k, 1)
-            to_x(k, 1, 0)
-            to_core(k, 0, 1, 0)
-            return
+            for dy in (0, 1):
+                arrived(0, 0, dy, dz)
+                to_x(0, dy, dz)
+                to_core(0, 0, dy, dz)
+
+    def close0():
         for dz in (0,) + zorder:
-            arrived(k, 0, 1, dz)
-            to_x(k, 1, dz)
-            to_core(k, 0, 1, dz)
-
-    def yz_forward(k):
-        for dz in zorder:
-            arrived(k, 0, 1, dz)
-            to_x(k, 1, dz)
-            to_core(k, 0, 1, dz)
-
-    def x_forward(k):
-        order = [(0, 0)] + ([(1, 0)] if k == 0 else [])
-        order += [(0, dz) for dz in zorder]
-        order += [(1, dz) for dz in ((0,) if k > 0 else ()) + zorder]
-        for dy, dz in order:
-            arrived(k, 1, dy, dz)
-            to_core(k, 1, dy, dz)
+            for dy in (0, 1):
+                arrived(0, 1, dy, dz)
+                to_core(0, 1, dy, dz)
 
     def bulk_wait(sem, blocks):
         ref = bin_.at[pl.ds(0, blocks * zw), :]
         pltpu.make_async_copy(ref, ref, sem).wait()
 
-    def finish(k):
-        pltpu.make_async_copy(own(k), place(k, 0, 0, 0), own_sem.at[k]).wait()
-        bulk_wait(core_sem.at[k], 4 * nz)
+    def finish(k, dxs=(0, 1)):
+        if 0 in dxs:
+            pltpu.make_async_copy(own(k), place(k, 0, 0, 0), own_sem.at[k]).wait()
+        for dx in dxs:
+            bulk_wait(core_sem.at[k, dx], 2 * nz)
 
     gcopy = rcopy(gain, gbuf, ms.at[3], mr.at[3], s, py)
     t0 = rcopy(tails.at[0], hbuf.at[0], ms.at[0], mr.at[0], s, py)
     nxt = lax.rem(s + 1, nsp)
     t1 = [rcopy(tails.at[1], hbuf.at[h], ms.at[1], mr.at[h], nxt, 0) for h in (0, 1)]
-    L = stream.shape[1]
-    d1 = rcopy(dcol.at[pl.ds(L - HALO, HALO), :], dbuf, ms.at[2], mr.at[2], nxt, 0)
+    d1 = rcopy(docs, dbuf, ms.at[2], mr.at[2], nxt, 0)
     more = s < nsp - 1
-    own_sends(0)
+    begin0()
     gcopy.start()
 
     @pl.when(y == 0)
@@ -237,8 +256,10 @@
     def turn(block):
         return block.astype(F32).T
 
-    y_forward(0)
-    own_sends(1)
+    across0()
+    for k in (1, 2, 3):
+        to_z(k, 0)
+        keep_own(k)
 
     @pl.loop(0, nb)
     def _(b):
@@ -248,7 +269,7 @@
     @pl.when(y == 1)
     def _():
         hbuf[1] = tails[0]
-        dbuf[...] = dcol[pl.ds(H - HALO, HALO), :]
+        dbuf[L // zw - 1:L // zw] = docs[H // zw - 1:H // zw]
 
     @pl.when(jnp.logical_and(y == 0, s == 0))
     def _():
@@ -265,8 +286,14 @@
         d1.wait_recv()
 
     gcopy.wait_recv()
-    docs_all = jnp.concatenate([dbuf[...], dcol[pl.ds(pl.multiple_of(y * H, H), H), :]], axis=0)
-    docs_f = docs_all.astype(F32)
+
+    def upright(row):
+        return jnp.broadcast_to(row.astype(F32), (zw, zw)).T
+
+    docs_f = jnp.concatenate(
+        [upright(dbuf[L // zw - 1:L // zw])[zw - HALO:]]
+        + [upright(jnp.where(y == 0, docs[i:i + 1], docs[H // zw + i:H // zw + i + 1])) for i in range(H // zw)],
+        axis=0)
     count = jnp.ones((T, 128), F32)
     for i in range(4):
         same = (pltpu.roll(docs_f, 1 << i, 0) == docs_f).astype(F32)
@@ -279,11 +306,10 @@
             at = (cc * 2 + xx) * seg + zz * zw
             res[pl.ds(0, HALO), at:at + zw] = hbuf[h, :, b * zw:(b + 1) * zw].astype(F32)
 
-    z_forward(0)
-    yz_forward(0)
-    z_forward(1)
-    own_sends(2)
-    x_forward(0)
+    along0()
+    for dz in (0,) + zorder:
+        first_hop(1, dz)
+    close0()
     per = chunk // zw
     for i in range(4):
         xs[i].wait_recv()
@@ -320,16 +346,17 @@
                     total = total + masks[i] * pltpu.roll(total, 1 << i, 0)
                 pooled[:, at] = (total * invs[g] - v).astype(BF16)
 
+    for dz in (0,) + zorder:
+        first_hop(2, dz)
     finish(0)
     norm(0)
     in_proj(0)
-    y_forward(1)
-    z_forward(2)
-    own_sends(3)
+    second_hop(1)
+    for dz in (0,) + zorder:
+        first_hop(3, dz)
     pool()
-    x_forward(1)
-    y_forward(2)
-    z_forward(3)
+    second_hop(2)
+    third_hop(1)
     finish(1)
 
     @pl.loop(0, 4)
@@ -339,45 +366,50 @@
         res[:, at] += jnp.dot(pooled[...], w, preferred_element_type=F32)
 
     norm(1)
-    x_forward(2)
-    y_forward(3)
+    second_hop(3)
+    third_hop(2)
     finish(2)
     in_proj(1)
     pool()
-    x_forward(3)
-    finish(3)
+    finish(3, (0,))
     hz = nz // 2
 
     def last(q, h):
         cols = pl.ds(pl.multiple_of(h * hz * zw, hz * zw), hz * zw)
-        w = bout[pl.ds((4 + q) * PW, PW), cols]
+        w = bout[pl.ds(pl.multiple_of((4 + q) * PW, PW), PW), cols]
         at = pl.ds(pl.multiple_of(q * seg + h * hz * zw, hz * zw), hz * zw)
         r = res[pl.ds(HALO, H), at] + jnp.dot(pooled[pl.ds(HALO, H), :], w, preferred_element_type=F32)
         return r.T.astype(BF16)
 
-    sends = []
-    pending = []
-    for q in range(4):
-        v = last(q, py)
-        for cp in pending:
-            cp.start()
-        pending = []
+    def part(dx, dc):
+        return lax.rem(c + dc, 2), lax.rem(x + dx, 2)
+
+    def outward(dx, dc):
+        cc, xx = part(dx, dc)
+        v = last(cc * 2 + xx, py)
         for i in range(hz):
-            b = i * 4 + (q % 2) * 2 + q // 2
-            ostage[b * zw:(b + 1) * zw, :] = v[i * zw:(i + 1) * zw, :]
-            pending.append(rcopy(
-                ostage.at[pl.ds(b * zw, zw), :],
-                out.at[pl.ds(b * zw, zw), pl.ds(pl.multiple_of(y * H, H), H)],
-                so.at[b], ro.at[b], s, py))
-        sends += pending
-    for q in range(4):
-        v = last(q, y)
-        for cp in pending:
-            cp.start()
-        pending = []
+            b = i * 4 + xx * 2 + cc
+            rows = pl.ds(pl.multiple_of(b * zw, zw), zw)
+            ostage[rows, :] = v[i * zw:(i + 1) * zw, :]
         for i in range(hz):
-            b = i * 4 + (q % 2) * 2 + q // 2
-            out[b * zw:(b + 1) * zw, pl.ds(pl.multiple_of(y * H, H), H)] = v[i * zw:(i + 1) * zw, :]
+            b = i * 4 + xx * 2 + cc
+            rows = pl.ds(pl.multiple_of(b * zw, zw), zw)
+            rcopy(ostage.at[rows, :], out.at[rows, pl.ds(pl.multiple_of(y * H, H), H)],
+                  so.at[b], ro.at[b], s, py).start()
+
+    outward(0, 0)
+    outward(0, 1)
+    third_hop(3)
+    finish(3, (1,))
+    outward(1, 0)
+    outward(1, 1)
+    for dx in (0, 1):
+        for dc in (0, 1):
+            cc, xx = part(dx, dc)
+            v = last(cc * 2 + xx, y)
+            for i in range(hz):
+                rows = pl.ds(pl.multiple_of((i * 4 + xx * 2 + cc) * zw, zw), zw)
+                out[rows, pl.ds(pl.multiple_of(y * H, H), H)] = v[i * zw:(i + 1) * zw, :]
 
     gcopy.wait_send()
 
@@ -409,7 +441,6 @@
     T = H + HALO
     nz = nsp // 4
     tails = jnp.stack([stream[:, H - HALO:H].T, stream[:, L - HALO:].T])
-    dcol = jnp.broadcast_to(docs[:, None], (L, 128))
     gain = norm_gain.reshape(LAYERS, rows // 128, 128)
     vmem = pl.BlockSpec(memory_space=pltpu.VMEM)
     dma = pltpu.SemaphoreType.DMA
@@ -428,16 +459,16 @@
             pltpu.VMEM((rows, H), BF16),
             pltpu.VMEM((rows, H), BF16),
             pltpu.VMEM((2, HALO, rows), BF16),
-            pltpu.VMEM((HALO, 128), jnp.int32),
+            pltpu.VMEM((L // 128, 128), jnp.int32),
             pltpu.VMEM((LAYERS, rows // 128, 128), F32),
             pltpu.VMEM((4, T, 128), F32),
             pltpu.VMEM((4, T, 128), F32),
-            dma((4, 4 * nz)), dma((4,)), dma((4,)), dma((4,)),
+            dma((4, 4 * nz)), dma((4, 2)), dma((4,)), dma((4,)),
             dma((4,)), dma((4,)), dma((rows // 128,)), dma((rows // 128,)),
             dma((4,)), dma((4,)),
         ],
         compiler_params=pltpu.CompilerParams(has_side_effects=True, vmem_limit_bytes=60 * 1024 * 1024),
-    )(stream, tails, dcol, gain, in_weight, out_weight)
+    )(stream, tails, docs.reshape(L // 128, 128), gain, in_weight, out_weight)
 
 
 def solution(mesh):

time: 147 us -> 139 us (0.946)
  Pallas kernels: 138 us -> 132 us
  local copies, waits for them, and re-layouts: 7.54 us -> 5.85 us
    pallas_call x1, Pallas kernels: 138 us -> 132 us  [fused_device(): pl.pallas_call(functools.partial(fused_kernel, nsp), out_shape=jax.ShapeD...]
    broadcast_in_dim x1 -> x0, local copies, waits for them, and re-layouts: 1.68 us -> none  [fused_device(): dcol = jnp.broadcast_to(docs[:, None], (L, 128))]
where the time goes in v2:
time: 139 us
  Pallas kernels  132 us (95%)
  local copies, waits for them, and re-layouts  5.85 us (4%)
    pallas_call x1, Pallas kernels, fused_device(): pl.pallas_call(functools.partial(fused_kernel, nsp), out_shape=jax.ShapeD...  132 us
    unnamed x4, local copies, waits for them, and re-layouts  4.61 us

profile of v2, /device:TPU:0, one launch (start us, length us, event | category | flops | bytes accessed | tf_op | source)
XLA Modules:
  0.0 138.7 jit_solution(12141657857736540099)
XLA Ops:
  0.0 1.3 copy.12
  1.3 1.2 fusion
  2.5 0.1 copy.8
  2.7 0.1 copy.9
  2.8 0.7 pad_maximum_fusion.tails
  3.5 132.2 %shard_map.55 = bf16[1024,1024]{1,0:T(8,128)(2,1)} custom-call(bf16[1024,1024]{1,0:T(8,128)(2,1)} %stream.1, bf16[2,32,1024]{2,1,0:T(8,128)(2,1)} %pad_maximum_fusion.tails, s32[8,128]{1,0:T(8,128)} %bitcast.15, f32[2,8,128]{2,1,0:T(8,128)} %bitcast.13, bf16[2,128,512]{2,1,0:T(8,128)(2,1)} %inw.1, bf16[2,512,128]{2,1,0:T(8,128)(2,1)} %outw.1), custom_call_target="tpu_custom_call" | custom-call | tf_op jit(solution)/shard_map/pallas_call | solution.py:447
  135.6 3.1 %copy.14 = bf16[1024,1024]{1,0:T(8,128)(2,1)} copy(bf16[1024,1024]{1,0:T(8,128)(2,1)} %shard_map.55) | data formatting | bytes 4194304
